TPU v7x, 32 devices: a whole 2x2x4 slice. The times are simulated.
32 devices in a mesh: rep: 2 (over x), fs: 8 (over z, y), tp: 2 (over core).
Axes of the slice: x: 2, y: 2, z: 4, core: 2. Of those that a mesh axis runs over, the one named last changes fastest.
Arguments:
- tokens: bfloat16 [5120, 2048], P(('rep', 'fs')), may hold values from -6 to 6
- mixer_out: bfloat16 [5120, 2048], P(('rep', 'fs')), may hold values from -6 to 6
- gate_first: bfloat16 [2048, 2816], P('fs', 'tp'), may hold values from -0.125 to 0.125
- up_first: bfloat16 [2048, 2816], P('fs', 'tp'), may hold values from -0.125 to 0.125
- down_first: bfloat16 [2816, 2048], P('tp', 'fs'), may hold values from -0.3125 to 0.3125
- gate_second: bfloat16 [2048, 2816], P('fs', 'tp'), may hold values from -0.125 to 0.125
- up_second: bfloat16 [2048, 2816], P('fs', 'tp'), may hold values from -0.125 to 0.125
- down_second: bfloat16 [2816, 2048], P('tp', 'fs'), may hold values from -0.3125 to 0.3125
- gain_first: float32 [2048], replicated, may hold values from 0.1 to 1.9
- bias_first: float32 [2048], replicated, may hold values from -1.5 to 1.5
- gain_middle: float32 [2048], replicated, may hold values from 0.1 to 1.9
- bias_middle: float32 [2048], replicated, may hold values from -1.5 to 1.5
- gain_last: float32 [2048], replicated, may hold values from 0.1 to 1.9
- bias_last: float32 [2048], replicated, may hold values from -1.5 to 1.5
Outputs:
- layer_out: bfloat16 [5120, 2048], P(('rep', 'fs'))
All inputs are finite; a program needn't handle non-finite values.
Results may differ from a plain program's by a relative error of at most 0.014.
Values may be sent and summed in bfloat16 or wider, within the bound.
A program may use at most 64 MiB of HBM per device.

v0:
```python
import functools
import math

import jax
import jax.numpy as jnp
from jax import lax
from jax.experimental import pallas as pl
from jax.experimental.pallas import tpu as pltpu
from jax.sharding import PartitionSpec as P

residual_scale = math.sqrt(2.0)
norm_eps = 1e-05
ZS, YS = 4, 2
F32, BF16 = jnp.float32, jnp.bfloat16


def normalize(summed, scaling, offset):
    center = summed - jnp.mean(summed, axis=-1, keepdims=True)
    spread = jnp.mean(center * center, axis=-1, keepdims=True)
    return center * lax.rsqrt(spread + norm_eps) * scaling + offset


def half_step(inputs, gate_weight, up_weight, down_weight):
    gate = jnp.dot(inputs, lax.all_gather(gate_weight, "fs", axis=0, tiled=True), preferred_element_type=F32)
    value = jnp.dot(inputs, lax.all_gather(up_weight, "fs", axis=0, tiled=True), preferred_element_type=F32)
    hidden = (jax.nn.silu(gate) * value).astype(BF16)
    partials = jnp.dot(hidden, lax.all_gather(down_weight, "fs", axis=1, tiled=True), preferred_element_type=F32)
    return lax.psum(partials.astype(BF16), "tp")


def per_device_general(
    tokens, mixer_out, gate_first, up_first, down_first, gate_second, up_second, down_second,
    gain_first, bias_first, gain_middle, bias_middle, gain_last, bias_last,
):
    first_branch = half_step(tokens, gate_first, up_first, down_first)
    first_norm = normalize(
        residual_scale * tokens.astype(F32) + 0.5 * first_branch.astype(F32), gain_first, bias_first
    ).astype(BF16)
    middle_norm = normalize(
        residual_scale * first_norm.astype(F32) + mixer_out.astype(F32), gain_middle, bias_middle
    ).astype(BF16)
    second_branch = half_step(middle_norm, gate_second, up_second, down_second)
    return normalize(
        residual_scale * middle_norm.astype(F32) + 0.5 * second_branch.astype(F32), gain_last, bias_last
    ).astype(BF16)


def slot(dz, dy):
    return (dz % ZS) * YS + dy % YS


SLOTS = ZS * YS
STEPS = range(1, ZS)
NAMES = [("y", 0, 0), ("y", 1, 0)] + [
    (way, d, dy) for way in ("up", "dn", "xup", "xdn") for d in STEPS for dy in range(YS)
]


def kernel(
    tokens_ref, mixer_ref, gu1_ref, gu2_ref, d1_ref, d2_ref,
    g1_ref, b1_ref, g2_ref, b2_ref, g3_ref, b3_ref,
    out_ref,
    gu, dn, xb, acc, hid, keep, psend, precv, xsend, xrecv, br, mix, fin,
    wsend, wrecv, xs_send, xs_recv, ds_send, ds_recv, rs_send, rs_recv, local,
):
    rep, fs, core = lax.axis_index("rep"), lax.axis_index("fs"), lax.axis_index("tp")
    z, y = fs // YS, fs % YS
    quarter = fin.shape[0]
    half_hidden = dn.shape[2]
    ks = gu.shape[2]
    dcols = dn.shape[3]

    def fs_of(dz, dy):
        return lax.rem(z + dz + ZS, ZS) * YS + lax.rem(y + dy, YS)

    def plane(dz, dy):
        return {"fs": fs_of(dz, dy)}

    other_rep, other_core, pair = {"rep": 1 - rep}, {"tp": 1 - core}, plane(0, 1)
    mine = pl.ds(pl.multiple_of(core * quarter, quarter), quarter)
    sib = pl.ds(pl.multiple_of((1 - core) * quarter, quarter), quarter)

    def hrows(who):
        return pl.ds(pl.multiple_of(who * half_hidden, half_hidden), half_hidden)

    own = slot(0, 0)
    loads = [
        pltpu.make_async_copy(gu1_ref.at[y], gu.at[0, own], local.at[0]),
        pltpu.make_async_copy(tokens_ref.at[mine], xb.at[0, pl.ds(0, quarter)], local.at[1]),
        pltpu.make_async_copy(tokens_ref.at[sib], xb.at[0, pl.ds(2 * quarter, quarter)], local.at[2]),
        pltpu.make_async_copy(d1_ref.at[hrows(y)], dn.at[0, own], local.at[3]),
        pltpu.make_async_copy(gu2_ref.at[y], gu.at[1, own], local.at[4]),
        pltpu.make_async_copy(d2_ref.at[hrows(y)], dn.at[1, own], local.at[5]),
        pltpu.make_async_copy(mixer_ref.at[mine], mix, local.at[6]),
    ]
    for load in loads:
        load.start()

    barrier = pltpu.get_barrier_semaphore()

    def greet(target):
        pl.semaphore_signal(barrier, inc=1, device_id=target, device_id_type=pl.DeviceIdType.MESH)

    for target in (pair, other_rep, other_core):
        greet(target)

    @pl.when(z < ZS - 1)
    def _():
        greet(plane(1, 0))

    @pl.when(z > 0)
    def _():
        greet(plane(-1, 0))

    inner = jnp.logical_and(z > 0, z < ZS - 1)

    @pl.when(inner)
    def _():
        pl.semaphore_wait(barrier, 5)

    @pl.when(jnp.logical_not(inner))
    def _():
        pl.semaphore_wait(barrier, 4)

    sent = []

    def remote(src, dst, send_sem, recv_sem, target):
        return pltpu.make_async_remote_copy(
            src_ref=src, dst_ref=dst, send_sem=send_sem, recv_sem=recv_sem,
            device_id=target, device_id_type=pl.DeviceIdType.MESH,
        )

    def send(copy):
        copy.start()
        sent.append(copy)

    weights = (gu.at[0], dn.at[0], gu.at[1], dn.at[1])

    def weight_copy(item, name):
        way, d, dy = name
        buf = weights[item]
        rows = buf.shape[1] // 2
        part = pl.ds(pl.multiple_of(rep * rows, rows), rows)
        sems = wsend.at[item, NAMES.index(name)], wrecv.at[item, NAMES.index(name)]
        if way == "y":
            at = rep if d == 0 else 1 - rep
            part = pl.ds(pl.multiple_of(at * rows, rows), rows)
            if item % 2 == 0:
                src = (gu1_ref, None, gu2_ref)[item].at[1 - y, part]
            else:
                first = (1 - y) * half_hidden + at * rows
                src = (None, d1_ref, None, d2_ref)[item].at[pl.ds(pl.multiple_of(first, rows), rows)]
            return remote(src, buf.at[slot(0, 1), part], *sems, pair)
        sign = -1 if way in ("up", "xup") else 1
        there = buf.at[slot(sign * d, dy), part]
        if way in ("xup", "xdn"):
            return remote(there, there, *sems, other_rep)
        return remote(buf.at[slot(sign * (d - 1), dy), part], there, *sems, plane(-sign, 0))

    def sends_up(d):
        return jnp.logical_and(z >= d - 1, z < ZS - 1)

    def sends_dn(d):
        return jnp.logical_and(z + d - 1 <= ZS - 1, z > 0)

    def gets_up(d):
        return z >= d

    def gets_dn(d):
        return z + d <= ZS - 1

    def line_start(item, d, dy):
        @pl.when(sends_up(d))
        def _():
            weight_copy(item, ("up", d, dy)).start()

        @pl.when(sends_dn(d))
        def _():
            weight_copy(item, ("dn", d, dy)).start()

    def relay(item, d, dy):
        for way, gets in (("up", gets_up), ("dn", gets_dn)):
            @pl.when(gets(d))
            def _():
                weight_copy(item, (way, d, dy)).wait_recv()
                if d < ZS - 1:
                    @pl.when((sends_up if way == "up" else sends_dn)(d + 1))
                    def _():
                        weight_copy(item, (way, d + 1, dy)).start()
                weight_copy(item, ("x" + way, d, dy)).start()

    def swapped(item, d):
        for way, gets in (("xup", gets_up), ("xdn", gets_dn)):
            @pl.when(gets(d))
            def _():
                for dy in range(YS):
                    weight_copy(item, (way, d, dy)).wait_recv()

    def pair_start(item, part):
        send(weight_copy(item, ("y", part, 0)))

    def pair_wait(item, part):
        weight_copy(item, ("y", part, 0)).wait_recv()

    def share_out(ffn):
        return remote(xb.at[ffn, pl.ds(0, quarter)], xb.at[ffn, pl.ds(quarter, quarter)],
                      xs_send.at[ffn], xs_recv.at[ffn], pair)

    def share_own(ffn):
        return remote(xb.at[ffn, pl.ds(0, quarter)], xb.at[ffn, pl.ds(2 * quarter, quarter)],
                      ds_send.at[ffn, 0], ds_recv.at[ffn, 0], other_core)

    def share_on(ffn):
        return remote(xb.at[ffn, pl.ds(quarter, quarter)], xb.at[ffn, pl.ds(3 * quarter, quarter)],
                      ds_send.at[ffn, 1], ds_recv.at[ffn, 1], other_core)

    def share_finish(ffn):
        share_out(ffn).wait_recv()
        send(share_on(ffn))
        if ffn:
            share_own(ffn).wait_recv()
        share_on(ffn).wait_recv()

    rows_step = 2 * quarter

    def gate_up_slot(ffn, dz, dy, first=False):
        n = slot(dz, 0) + dy
        cols = pl.ds(pl.multiple_of(fs_of(dz, dy) * ks, ks), ks)

        @pl.loop(0, 2)
        def _(i):
            rows = pl.ds(pl.multiple_of(i * rows_step, rows_step), rows_step)
            part = jnp.dot(xb[ffn, rows, cols], gu[ffn, n], preferred_element_type=F32)
            if first:
                acc[rows, :] = part
            else:
                acc[rows, :] += part

    def at_distance(d, act):
        for dz, gets in ((-d, gets_up), (d, gets_dn)):
            @pl.when(gets(d))
            def _():
                @pl.loop(0, YS)
                def _(dy):
                    act(dz, dy)

    def activate():
        low = half_hidden // 128 * 128
        wide = acc.shape[1] - low

        @pl.loop(0, 4 * quarter // 32)
        def _(i):
            rows = pl.ds(pl.multiple_of(i * 32, 32), 32)
            gate = acc[rows, :wide]
            value = acc[rows, low:]
            if half_hidden != low:
                value = pltpu.roll(value, wide - (half_hidden - low), axis=1)
            made = gate / (1.0 + jnp.exp(-gate)) * value
            hid[rows, :] = made[:, :half_hidden].astype(BF16)

    def to_sibling(ffn, n):
        return remote(psend.at[ffn, n], precv.at[ffn, n], rs_send.at[ffn, 0, n], rs_recv.at[ffn, 0, n], other_core)

    def to_pair(ffn, dz, dy):
        n, there = slot(dz, 0) + dy, slot(dz, 0) + 1 - dy
        return remote(xsend.at[ffn, n], xrecv.at[ffn, there], rs_send.at[ffn, 1, n], rs_recv.at[ffn, 1, there], pair)

    def from_pair(ffn, n):
        return remote(xsend.at[ffn, n], xrecv.at[ffn, n], rs_send.at[ffn, 1, n], rs_recv.at[ffn, 1, n], pair)

    def down_slot(ffn, dz, dy):
        n = slot(dz, 0) + dy
        whole = jnp.dot(hid[2 * quarter:, :], dn[ffn, n], preferred_element_type=F32)
        psend[ffn, n] = whole.astype(BF16)
        keep[n] = jnp.dot(hid[:2 * quarter, :], dn[ffn, n], preferred_element_type=F32)
        to_sibling(ffn, n).start()

    def add_cores(ffn, dz, dy):
        n = slot(dz, 0) + dy
        to_sibling(ffn, n).wait_recv()
        xsend[ffn, n] = (keep[n, quarter:, :] + precv[ffn, n, quarter:, :].astype(F32)).astype(BF16)
        keep[n, :quarter, :] = keep[n, :quarter, :] + precv[ffn, n, :quarter, :].astype(F32)
        to_pair(ffn, dz, dy).start()

    def collect_slot(ffn, dz, dy):
        n = slot(dz, 0) + dy
        from_pair(ffn, n).wait_recv()
        cols = pl.ds(pl.multiple_of(fs_of(dz, dy) * dcols, dcols), dcols)
        br[:, cols] = keep[n, :quarter, :] + xrecv[ffn, n].astype(F32)

    def first_norms():
        @pl.loop(0, quarter // 16)
        def _(i):
            rows = pl.ds(pl.multiple_of(i * 16, 16), 16)
            first = normalize(
                residual_scale * xb[0, rows, :].astype(F32) + 0.5 * br[rows, :], g1_ref[...], b1_ref[...]
            ).astype(BF16)
            xb[1, rows, :] = normalize(
                residual_scale * first.astype(F32) + mix[rows, :].astype(F32), g2_ref[...], b2_ref[...]
            ).astype(BF16)

    def last_norm():
        @pl.loop(0, quarter // 16)
        def _(i):
            rows = pl.ds(pl.multiple_of(i * 16, 16), 16)
            fin[rows, :] = normalize(
                residual_scale * xb[1, rows, :].astype(F32) + 0.5 * br[rows, :], g3_ref[...], b3_ref[...]
            ).astype(BF16)

    def open_item(item):
        pair_start(item, 0)
        loads[(0, 3, 4, 5)[item]].wait()
        line_start(item, 1, 0)

    def second_start(item):
        pair_wait(item, 0)
        line_start(item, 1, 1)

    def work(item, d):
        ffn = item // 2
        if item % 2 == 0:
            at_distance(d, lambda dz, dy: gate_up_slot(ffn, dz, dy))
        else:
            at_distance(d, lambda dz, dy: down_slot(ffn, dz, dy))
            at_distance(d, lambda dz, dy: add_cores(ffn, dz, dy))

    def work_near(item, dy):
        ffn = item // 2
        if item % 2 == 0:
            gate_up_slot(ffn, 0, dy, first=dy == 0)
        else:
            down_slot(ffn, 0, dy)
            add_cores(ffn, 0, dy)

    def finish(item):
        ffn = item // 2
        for d in range(2, ZS):
            swapped(item, d)
            work(item, d)
        if item % 2 == 0:
            activate()
        else:
            for dy in range(YS):
                collect_slot(ffn, 0, dy)
            for d in STEPS:
                at_distance(d, lambda dz, dy: collect_slot(ffn, dz, dy))

    for item in range(4):
        if item == 0:
            open_item(0)
            loads[1].wait()
            send(share_out(0))
            pair_start(0, 1)
            second_start(0)
        relay(item, 1, 0)
        if item:
            finish(item - 1)
        if item == 2:
            loads[6].wait()
            first_norms()
            send(share_out(1))
            send(share_own(1))
            pair_start(2, 1)
        relay(item, 1, 1)
        if item == 0:
            loads[2].wait()
            share_finish(0)
        if item != 2:
            work_near(item, 0)
            pair_wait(item, 1)
            work_near(item, 1)
        for dy in range(YS):
            relay(item, 2, dy)
        if item < 3:
            open_item(item + 1)
            if item + 1 != 2:
                pair_start(item + 1, 1)
        if item == 2:
            share_finish(1)
            work_near(2, 0)
            pair_wait(2, 1)
            work_near(2, 1)
        relay(item, 3, 0)
        if item < 3:
            second_start(item + 1)
        swapped(item, 1)
        work(item, 1)
        relay(item, 3, 1)
    finish(3)
    last_norm()
    put = pltpu.make_async_copy(fin, out_ref.at[mine], local.at[7])
    put.start()
    over = remote(fin, out_ref.at[mine], ds_send.at[0, 0], ds_recv.at[0, 0], other_core)
    over.start()
    over.wait()
    put.wait()
    for copy in sent:
        copy.wait_send()
    for ffn in range(2):
        for n in range(SLOTS):
            to_sibling(ffn, n).wait_send()
            from_pair(ffn, n).wait_send()
    for item in range(4):
        for d in STEPS:
            for way, does in (("up", sends_up), ("dn", sends_dn), ("xup", gets_up), ("xdn", gets_dn)):
                @pl.when(does(d))
                def _():
                    for dy in range(YS):
                        weight_copy(item, (way, d, dy)).wait_send()


def per_device(
    tokens, mixer_out, gate_first, up_first, down_first, gate_second, up_second, down_second,
    gain_first, bias_first, gain_middle, bias_middle, gain_last, bias_last,
):
    rows, width = tokens.shape
    ks, hidden = gate_first.shape
    half_hidden = hidden // 2
    dcols = down_first.shape[1]
    quarter = rows // 2

    def halves(gate, up):
        return jnp.stack(
            [
                jnp.concatenate([w[:, at:at + half_hidden] for w in (gate, up)], axis=1)
                for at in (0, half_hidden)
            ]
        )

    any_spec, vmem = pl.BlockSpec(memory_space=pl.ANY), pl.BlockSpec(memory_space=pltpu.VMEM)
    vec = lambda v: v.reshape(1, width)
    dma = pltpu.SemaphoreType.DMA
    return pl.pallas_call(
        kernel,
        out_shape=jax.ShapeDtypeStruct((rows, width), BF16),
        in_specs=[any_spec] * 6 + [vmem] * 6,
        out_specs=any_spec,
        scratch_shapes=[
            pltpu.VMEM((2, SLOTS, ks, hidden), BF16),
            pltpu.VMEM((2, SLOTS, half_hidden, dcols), BF16),
            pltpu.VMEM((2, 4 * quarter, width), BF16),
            pltpu.VMEM((4 * quarter, hidden), F32),
            pltpu.VMEM((4 * quarter, half_hidden), BF16),
            pltpu.VMEM((SLOTS, 2 * quarter, dcols), F32),
            pltpu.VMEM((2, SLOTS, 2 * quarter, dcols), BF16),
            pltpu.VMEM((2, SLOTS, 2 * quarter, dcols), BF16),
            pltpu.VMEM((2, SLOTS, quarter, dcols), BF16),
            pltpu.VMEM((2, SLOTS, quarter, dcols), BF16),
            pltpu.VMEM((quarter, width), F32),
            pltpu.VMEM((quarter, width), BF16),
            pltpu.VMEM((quarter, width), BF16),
            dma((4, len(NAMES))), dma((4, len(NAMES))),
            dma((2,)), dma((2,)),
            dma((2, 2)), dma((2, 2)),
            dma((2, 2, SLOTS)), dma((2, 2, SLOTS)),
            dma((8,)),
        ],
        compiler_params=pltpu.CompilerParams(
            collective_id=0, has_side_effects=True, vmem_limit_bytes=60 * 1024 * 1024
        ),
    )(
        tokens, mixer_out, halves(gate_first, up_first), halves(gate_second, up_second),
        down_first, down_second,
        vec(gain_first), vec(bias_first), vec(gain_middle), vec(bias_middle), vec(gain_last), vec(bias_last),
    )


def on_mesh(mesh, rows, width, hidden):
    sizes = dict(mesh.shape)
    if (sizes["rep"], sizes["fs"], sizes["tp"]) != (2, SLOTS, 2):
        return False
    rows, ks, hidden = rows // (2 * SLOTS), width // SLOTS, hidden // 2
    return rows % 32 == 0 and ks % 128 == 0 and hidden % 128 == 0 and (hidden // 2) % 64 == 0


def solution(mesh):
    def run(tokens, mixer_out, gate_first, *rest):
        fits = on_mesh(mesh, tokens.shape[0], tokens.shape[1], gate_first.shape[1])
        return jax.shard_map(
            per_device if fits else per_device_general,
            mesh=mesh,
            in_specs=(
                P(("rep", "fs"), None), P(("rep", "fs"), None),
                P("fs", "tp"), P("fs", "tp"), P("tp", "fs"),
                P("fs", "tp"), P("fs", "tp"), P("tp", "fs"),
                P(), P(), P(), P(), P(), P(),
            ),
            out_specs=P(("rep", "fs"), None),
            check_vma=False,
        )(tokens, mixer_out, gate_first, *rest)

    return run
```

profile of v0, /device:TPU:0, one launch (start us, length us, event | category | flops | bytes accessed | tf_op | source)
XLA Modules:
  0.0 193.6 jit_solution(3283093862302236219)
XLA Ops:
  0.0 0.0 copy-start
  0.0 1.4 fusion.2
  1.4 0.0 copy-done
  1.4 0.2 fusion.3
  1.6 0.4 maximum_bitcast_fusion
  2.0 0.0 copy-start.1
  2.0 1.3 pad_maximum_fusion.gu1_ref
  3.3 0.0 copy-done.1
  3.3 0.0 copy-start.2
  3.3 0.2 fusion
  3.4 0.9 copy-done.2
  4.4 0.2 fusion.1
  4.6 0.4 maximum_bitcast_fusion.2
  5.0 1.3 pad_maximum_fusion.1.gu2_ref
  6.2 184.9 %shard_map.136 = bf16[320,2048]{1,0:T(8,128)(2,1)} custom-call(bf16[320,2048]{1,0:T(8,128)(2,1)} %tokens_ref.1, bf16[320,2048]{1,0:T(8,128)(2,1)} %mixer_ref.1, bf16[2,256,1408]{2,1,0:T(8,128)(2,1)} %pad_maximum_fusion.gu1_ref, bf16[2,256,1408]{2,1,0:T(8,128)(2,1)} %pad_maximum_fusion.1.gu2_ref, bf16[1408,256]{1,0:T(8,128)(2,1)} %d1_ref.1, ...), custom_call_target="tpu_custom_call" | custom-call | tf_op jit(solution)/shard_map/pallas_call | solution.py:433
  191.1 2.5 %copy.16 = bf16[320,2048]{1,0:T(8,128)(2,1)} copy(bf16[320,2048]{1,0:T(8,128)(2,1)} %shard_map.136) | data formatting | bytes 2621440
Async XLA Ops:
  0.0 1.4 copy-start
  2.0 1.3 copy-start.1
  3.3 1.1 copy-start.2
where the time goes:
time: 194 us
  Pallas kernels  185 us (95%)
  local copies, waits for them, and re-layouts  5.33 us (3%)
  other arithmetic  3.38 us (2%)
    pallas_call x1, Pallas kernels, per_device(): pl.pallas_call(kernel, out_shape=jax.ShapeDtypeStruct((rows, width), BF16...  185 us

commit v1 on v0

v1 whole, which is shorter than its diff:
```python
import math

import jax
import jax.numpy as jnp
from jax import lax
from jax.experimental import pallas as pl
from jax.experimental.pallas import tpu as pltpu
from jax.sharding import PartitionSpec as P

residual_scale = math.sqrt(2.0)
norm_eps = 1e-05
ZS, YS = 4, 2
F32, BF16 = jnp.float32, jnp.bfloat16


def normalize(summed, scaling, offset):
    center = summed - jnp.mean(summed, axis=-1, keepdims=True)
    spread = jnp.mean(center * center, axis=-1, keepdims=True)
    return center * lax.rsqrt(spread + norm_eps) * scaling + offset


def half_step(inputs, gate_weight, up_weight, down_weight):
    gate = jnp.dot(inputs, lax.all_gather(gate_weight, "fs", axis=0, tiled=True), preferred_element_type=F32)
    value = jnp.dot(inputs, lax.all_gather(up_weight, "fs", axis=0, tiled=True), preferred_element_type=F32)
    hidden = (jax.nn.silu(gate) * value).astype(BF16)
    partials = jnp.dot(hidden, lax.all_gather(down_weight, "fs", axis=1, tiled=True), preferred_element_type=F32)
    return lax.psum(partials.astype(BF16), "tp")


def per_device_general(
    tokens, mixer_out, gate_first, up_first, down_first, gate_second, up_second, down_second,
    gain_first, bias_first, gain_middle, bias_middle, gain_last, bias_last,
):
    first_branch = half_step(tokens, gate_first, up_first, down_first)
    first_norm = normalize(
        residual_scale * tokens.astype(F32) + 0.5 * first_branch.astype(F32), gain_first, bias_first
    ).astype(BF16)
    middle_norm = normalize(
        residual_scale * first_norm.astype(F32) + mixer_out.astype(F32), gain_middle, bias_middle
    ).astype(BF16)
    second_branch = half_step(middle_norm, gate_second, up_second, down_second)
    return normalize(
        residual_scale * middle_norm.astype(F32) + 0.5 * second_branch.astype(F32), gain_last, bias_last
    ).astype(BF16)


def slot_of(step):
    return step % ZS


STEPS = range(1, ZS)
WAYS = [(way, d, dy) for way in ("up", "dn") for d in STEPS for dy in range(YS)]
MAIN, EXTRA, DOWN = range(3)
GATE_UP = (MAIN, EXTRA)


def kernel(
    tokens_ref, mixer_ref, g1_ref, u1_ref, e1_ref, d1_ref, g2_ref, u2_ref, e2_ref, d2_ref,
    gain1_ref, bias1_ref, gain2_ref, bias2_ref, gain3_ref, bias3_ref,
    out_ref,
    gum, gux, dn, xb, acc, low, high, hid, keep, psend, precv, xsend, xrecv, ysend, yrecv, br, mix, fin,
    zs_send, zs_recv, ys_send, ys_recv, ag_send, ag_recv, rs_send, rs_recv, fin_send, fin_recv, local,
):
    rep, fs, core = lax.axis_index("rep"), lax.axis_index("fs"), lax.axis_index("tp")
    z, y = fs // YS, fs % YS
    quarter = fin.shape[0]
    half = 4 * quarter
    ks = gum.shape[2] // YS
    main = gum.shape[3] // 2
    fold = gux.shape[2] // YS
    extra = gux.shape[3] // 4
    wide = low.shape[1]
    dcols = dn.shape[3]
    own_q, pair_q = rep * YS + y, rep * YS + 1 - y

    pair = {"fs": z * YS + 1 - y}
    other_core = {"tp": 1 - core}
    near = {"rep": lax.rem(rep + core, 2), "fs": z * YS + lax.rem(y + 1 - core, YS)}
    far = {"rep": lax.rem(rep + 1 - core, 2), "fs": z * YS + lax.rem(y + core, YS)}

    def ds(first, count, unit):
        return pl.ds(pl.multiple_of(first, unit), count)

    mine, sib = ds(core * quarter, quarter, quarter), ds((1 - core) * quarter, quarter, quarter)
    weights = ((g1_ref, u1_ref, e1_ref, d1_ref), (g2_ref, u2_ref, e2_ref, d2_ref))

    def pieces(f, q):
        gate, up, ex, down = weights[f]
        rows, mrows, ex_rows = ds(y * ks, ks, ks), ds(q * main, main, main), ds(4 * main + q * extra, extra, 32)
        return (
            (gate.at[:, ds(q * main, main, main)], gum.at[f, 0, rows, pl.ds(0, main)]),
            (up.at[:, ds(q * main, main, main)], gum.at[f, 0, rows, pl.ds(main, main)]),
            (ex.at[q], gux.at[f, 0, ds(y * fold, fold, fold)]),
            (down.at[mrows], dn.at[f, y, pl.ds(0, main)]),
            (down.at[ex_rows], dn.at[f, y, pl.ds(main, extra)]),
        )

    loads = [
        [pltpu.make_async_copy(src, dst, local.at[5 * f + i]) for i, (src, dst) in enumerate(pieces(f, own_q))]
        for f in range(2)
    ]
    token_loads = [
        pltpu.make_async_copy(tokens_ref.at[mine], xb.at[0, pl.ds(0, quarter)], local.at[10]),
        pltpu.make_async_copy(tokens_ref.at[sib], xb.at[0, pl.ds(half, quarter)], local.at[11]),
    ]
    mixer_load = pltpu.make_async_copy(mixer_ref.at[mine], mix, local.at[12])
    for load in loads[0][:3] + token_loads + loads[0][3:] + loads[1] + [mixer_load]:
        load.start()

    barrier = pltpu.get_barrier_semaphore()

    def greet(target):
        pl.semaphore_signal(barrier, inc=1, device_id=target, device_id_type=pl.DeviceIdType.MESH)

    def plane(dz):
        return {"fs": lax.rem(z + dz + ZS, ZS) * YS + y}

    for target in (near, far, other_core):
        greet(target)

    @pl.when(z < ZS - 1)
    def _():
        greet(plane(1))

    @pl.when(z > 0)
    def _():
        greet(plane(-1))

    inner = jnp.logical_and(z > 0, z < ZS - 1)

    @pl.when(inner)
    def _():
        pl.semaphore_wait(barrier, 5)

    @pl.when(jnp.logical_not(inner))
    def _():
        pl.semaphore_wait(barrier, 4)

    sent = []

    def remote(src, dst, send_sem, recv_sem, target):
        return pltpu.make_async_remote_copy(
            src_ref=src, dst_ref=dst, send_sem=send_sem, recv_sem=recv_sem,
            device_id=target, device_id_type=pl.DeviceIdType.MESH,
        )

    def send(copy):
        copy.start()
        sent.append(copy)

    def pair_copy(f, i):
        src, dst = pieces(f, pair_q)[i]
        return remote(src, dst, ys_send.at[f, i], ys_recv.at[f, i], pair)

    def pair_landing(f, i):
        gate_rows = ds((1 - y) * ks, ks, ks)
        dst = (
            gum.at[f, 0, gate_rows, pl.ds(0, main)], gum.at[f, 0, gate_rows, pl.ds(main, main)],
            gux.at[f, 0, ds((1 - y) * fold, fold, fold)],
            dn.at[f, 1 - y, pl.ds(0, main)], dn.at[f, 1 - y, pl.ds(main, extra)],
        )[i]
        return remote(dst, dst, ys_send.at[f, i], ys_recv.at[f, i], pair)

    def pair_start(f, which):
        for i in which:
            send(pair_copy(f, i))

    def pair_wait(f, which):
        for i in which:
            pair_landing(f, i).wait_recv()

    def z_copy(f, piece, name):
        way, d, dy = name
        ya = lax.rem(y + dy, YS)
        sign = -1 if way == "up" else 1

        def at(n):
            if piece == MAIN:
                return gum.at[f, n, ds(ya * ks, ks, ks)]
            if piece == EXTRA:
                return gux.at[f, n, ds(ya * fold, fold, fold)]
            return dn.at[f, n * YS + ya]

        sems = zs_send.at[f, piece, WAYS.index(name)], zs_recv.at[f, piece, WAYS.index(name)]
        return remote(at(slot_of(sign * (d - 1))), at(slot_of(sign * d)), *sems, plane(-sign))

    def sends_up(d):
        return jnp.logical_and(z >= d - 1, z < ZS - 1)

    def sends_dn(d):
        return jnp.logical_and(z + d - 1 <= ZS - 1, z > 0)

    def gets_up(d):
        return z >= d

    def gets_dn(d):
        return z + d <= ZS - 1

    def own_send(f, which, dy):
        for way, does in (("up", sends_up), ("dn", sends_dn)):
            @pl.when(does(1))
            def _():
                for piece in which:
                    z_copy(f, piece, (way, 1, dy)).start()

    def relay(f, which, d, dys=range(YS)):
        for dy in dys:
            for way, gets, does in (("up", gets_up, sends_up), ("dn", gets_dn, sends_dn)):
                @pl.when(gets(d))
                def _():
                    for piece in which:
                        z_copy(f, piece, (way, d, dy)).wait_recv()
                        if d < ZS - 1:
                            @pl.when(does(d + 1))
                            def _():
                                z_copy(f, piece, (way, d + 1, dy)).start()

    def gather(f, i):
        target = (near, far, far)[i] if i < 3 else other_core
        src = (0, 0, 1)[i] if i < 3 else i - 3
        dst = i + 1 if i < 3 else i + 1
        return remote(
            xb.at[f, pl.ds(src * quarter, quarter)], xb.at[f, pl.ds(dst * quarter, quarter)],
            ag_send.at[f, i], ag_recv.at[f, i], target,
        )

    def gather_start(f):
        send(gather(f, 0))
        send(gather(f, 1))
        if f:
            send(gather(f, 3))

    def gather_near(f):
        gather(f, 0).wait_recv()
        send(gather(f, 2))
        send(gather(f, 4))

    def gather_far(f):
        gather(f, 1).wait_recv()
        send(gather(f, 5))
        gather(f, 2).wait_recv()
        send(gather(f, 6))

    def gather_wait(f):
        for i in range(3 if f else 4, 7):
            gather(f, i).wait_recv()

    step = 2 * quarter

    def gate_up(f, dz, first=False):
        n, zz = lax.rem(dz + ZS, ZS), z + dz
        base = zz * YS * ks

        @pl.loop(0, 4)
        def _(i):
            rows = ds(i * step, step, step)
            folded = [
                jnp.concatenate(
                    [xb[f, rows, ds(base + at * ks + h * fold, fold, fold)] for at in range(YS)], axis=1
                )
                for h in range(2)
            ]
            parts = (
                (acc, jnp.dot(xb[f, rows, ds(base, YS * ks, YS * ks)], gum[f, n], preferred_element_type=F32)),
                (low, jnp.dot(folded[0], gux[f, n, :, :wide], preferred_element_type=F32)),
                (high, jnp.dot(folded[1], gux[f, n, :, 4 * extra - wide:], preferred_element_type=F32)),
            )
            for total, part in parts:
                if first:
                    total[rows, :] = part
                else:
                    total[rows, :] += part

    def at_distance(d, act):
        if d == 0:
            act(0)
            return

        @pl.loop(0, 2)
        def _(i):
            dz = (2 * i - 1) * d

            @pl.when(jnp.logical_and(z + dz >= 0, z + dz < ZS))
            def _():
                act(dz)

    def both(d, act):
        def slots(dz):
            @pl.loop(0, YS)
            def _(ya):
                act(dz, ya)

        at_distance(d, slots)

    def gated(gate, value):
        return gate / (1.0 + jnp.exp(-gate)) * value

    def activate():
        shift = 2 * extra - (4 * extra - wide)
        some = -(-extra // 128) * 128

        @pl.loop(0, 8 * quarter // 32)
        def _(i):
            rows = ds(i * 32, 32, 32)
            hid[rows, :main] = gated(acc[rows, :main], acc[rows, main:]).astype(BF16)
            rest = low[rows, :] + pltpu.roll(high[rows, :], wide - shift, axis=1)
            value = pltpu.roll(rest, wide - extra, axis=1)
            made = gated(rest[:, :some], value[:, :some])
            hid[rows, main:] = made[:, :extra].astype(BF16)

    def index(dz, ya):
        return lax.rem(dz + ZS, ZS) * YS + ya

    def to_sibling(f, n):
        return remote(psend.at[f, n], precv.at[f, n], rs_send.at[f, 0, n], rs_recv.at[f, 0, n], other_core)

    def to_far(f, n):
        return remote(xsend.at[f, n], xrecv.at[f, n], rs_send.at[f, 1, n], rs_recv.at[f, 1, n], far)

    def to_near(f, n):
        return remote(ysend.at[f, n], yrecv.at[f, n], rs_send.at[f, 2, n], rs_recv.at[f, 2, n], near)

    def down_slot(f, dz, ya):
        n = index(dz, ya)
        psend[f, n] = jnp.dot(hid[half:, :], dn[f, n], preferred_element_type=F32).astype(BF16)
        to_sibling(f, n).start()
        keep[n] = jnp.dot(hid[:half, :], dn[f, n], preferred_element_type=F32)

    def add_cores(f, dz, ya):
        n = index(dz, ya)
        to_sibling(f, n).wait_recv()
        xsend[f, n] = (keep[n, 2 * quarter:, :] + precv[f, n, 2 * quarter:, :].astype(F32)).astype(BF16)
        to_far(f, n).start()
        keep[n, :2 * quarter, :] = keep[n, :2 * quarter, :] + precv[f, n, :2 * quarter, :].astype(F32)

    def add_far(f, dz, ya):
        n = index(dz, ya)
        to_far(f, n).wait_recv()
        ysend[f, n] = (keep[n, quarter:2 * quarter, :] + xrecv[f, n, quarter:, :].astype(F32)).astype(BF16)
        to_near(f, n).start()
        keep[n, :quarter, :] = keep[n, :quarter, :] + xrecv[f, n, :quarter, :].astype(F32)

    def add_near(f, dz, ya):
        n = index(dz, ya)
        to_near(f, n).wait_recv()
        cols = ds(((z + dz) * YS + ya) * dcols, dcols, dcols)
        br[:, cols] = keep[n, :quarter, :] + yrecv[f, n].astype(F32)

    def down(f, d):
        both(d, lambda dz, ya: down_slot(f, dz, ya))
        both(d, lambda dz, ya: add_cores(f, dz, ya))

    def first_norms():
        @pl.loop(0, quarter // 16)
        def _(i):
            rows = ds(i * 16, 16, 16)
            first = normalize(
                residual_scale * xb[0, rows, :].astype(F32) + 0.5 * br[rows, :], gain1_ref[...], bias1_ref[...]
            ).astype(BF16)
            xb[1, rows, :] = normalize(
                residual_scale * first.astype(F32) + mix[rows, :].astype(F32), gain2_ref[...], bias2_ref[...]
            ).astype(BF16)

    def last_norm():
        @pl.loop(0, quarter // 16)
        def _(i):
            rows = ds(i * 16, 16, 16)
            fin[rows, :] = normalize(
                residual_scale * xb[1, rows, :].astype(F32) + 0.5 * br[rows, :], gain3_ref[...], bias3_ref[...]
            ).astype(BF16)

    def load_wait(f, which):
        for i in which:
            loads[f][i].wait()

    pair_start(0, range(3))
    load_wait(0, range(3))
    own_send(0, GATE_UP, 0)
    token_loads[0].wait()
    gather_start(0)
    pair_start(0, (3, 4))
    load_wait(0, (3, 4))
    own_send(0, (DOWN,), 0)
    pair_wait(0, range(3))
    own_send(0, GATE_UP, 1)
    relay(0, GATE_UP, 1, (0,))
    gather_near(0)
    relay(0, GATE_UP, 1, (1,))
    gather_far(0)
    pair_start(1, range(3))
    token_loads[1].wait()
    gather_wait(0)
    gate_up(0, 0, first=True)
    relay(0, GATE_UP, 2, (0,))
    at_distance(1, lambda dz: gate_up(0, dz))
    relay(0, GATE_UP, 2, (1,))
    pair_wait(0, (3, 4))
    own_send(0, (DOWN,), 1)
    relay(0, (DOWN,), 1)
    pair_start(1, (3, 4))
    at_distance(2, lambda dz: gate_up(0, dz))
    relay(0, GATE_UP, 3)
    at_distance(3, lambda dz: gate_up(0, dz))
    relay(0, (DOWN,), 2)
    load_wait(1, range(5))
    own_send(1, GATE_UP, 0)
    pair_wait(1, range(3))
    own_send(1, GATE_UP, 1)
    for f in range(2):
        activate()
        down(f, 0)
        down(f, 1)
        both(0, lambda dz, ya: add_far(f, dz, ya))
        down(f, 2)
        both(1, lambda dz, ya: add_far(f, dz, ya))
        both(0, lambda dz, ya: add_near(f, dz, ya))
        relay(f, (DOWN,), 3)
        down(f, 3)
        both(2, lambda dz, ya: add_far(f, dz, ya))
        both(1, lambda dz, ya: add_near(f, dz, ya))
        both(3, lambda dz, ya: add_far(f, dz, ya))
        both(2, lambda dz, ya: add_near(f, dz, ya))
        both(3, lambda dz, ya: add_near(f, dz, ya))
        if f == 0:
            mixer_load.wait()
            first_norms()
            gather_start(1)
            relay(1, GATE_UP, 1)
            gather_near(1)
            relay(1, GATE_UP, 2)
            own_send(1, (DOWN,), 0)
            pair_wait(1, (3, 4))
            own_send(1, (DOWN,), 1)
            gather_far(1)
            gather_wait(1)
            gate_up(1, 0, first=True)
            at_distance(1, lambda dz: gate_up(1, dz))
            relay(1, (DOWN,), 1)
            at_distance(2, lambda dz: gate_up(1, dz))
            relay(1, (DOWN,), 2)
            relay(1, GATE_UP, 3)
            at_distance(3, lambda dz: gate_up(1, dz))
    last_norm()
    put = pltpu.make_async_copy(fin, out_ref.at[mine], local.at[13])
    put.start()
    over = remote(fin, out_ref.at[mine], fin_send.at[0], fin_recv.at[0], other_core)
    over.start()
    over.wait()
    put.wait()
    for copy in sent:
        copy.wait_send()
    for f in range(2):
        @pl.loop(0, ZS * YS)
        def _(n):
            for copy in (to_sibling(f, n), to_far(f, n), to_near(f, n)):
                copy.wait_send()

        for d in STEPS:
            for way, does in (("up", sends_up), ("dn", sends_dn)):
                @pl.when(does(d))
                def _():
                    for piece in range(3):
                        for dy in range(YS):
                            z_copy(f, piece, (way, d, dy)).wait_send()


def per_device(
    tokens, mixer_out, gate_first, up_first, down_first, gate_second, up_second, down_second,
    gain_first, bias_first, gain_middle, bias_middle, gain_last, bias_last,
):
    rows, width = tokens.shape
    ks, hidden = gate_first.shape
    dcols = down_first.shape[1]
    quarter = rows // 2
    main, extra = split(hidden)
    wide = -(-2 * extra // 128) * 128
    slots = ZS * YS

    def leftovers(gate, up):
        def part(w, h, q):
            return w[h * (ks // 2):(h + 1) * (ks // 2), 4 * main + q * extra:4 * main + (q + 1) * extra]

        return jnp.stack([
            jnp.concatenate([part(w, h, q) for h in range(2) for w in (gate, up)], axis=1) for q in range(4)
        ])

    any_spec, vmem = pl.BlockSpec(memory_space=pl.ANY), pl.BlockSpec(memory_space=pltpu.VMEM)
    vec = lambda v: v.reshape(1, width)
    dma = pltpu.SemaphoreType.DMA
    return pl.pallas_call(
        kernel,
        out_shape=jax.ShapeDtypeStruct((rows, width), BF16),
        in_specs=[any_spec] * 10 + [vmem] * 6,
        out_specs=any_spec,
        scratch_shapes=[
            pltpu.VMEM((2, ZS, YS * ks, 2 * main), BF16),
            pltpu.VMEM((2, ZS, YS * ks // 2, 4 * extra), BF16),
            pltpu.VMEM((2, slots, main + extra, dcols), BF16),
            pltpu.VMEM((2, 8 * quarter, width), BF16),
            pltpu.VMEM((8 * quarter, 2 * main), F32),
            pltpu.VMEM((8 * quarter, wide), F32),
            pltpu.VMEM((8 * quarter, wide), F32),
            pltpu.VMEM((8 * quarter, main + extra), BF16),
            pltpu.VMEM((slots, 4 * quarter, dcols), F32),
            pltpu.VMEM((2, slots, 4 * quarter, dcols), BF16),
            pltpu.VMEM((2, slots, 4 * quarter, dcols), BF16),
            pltpu.VMEM((2, slots, 2 * quarter, dcols), BF16),
            pltpu.VMEM((2, slots, 2 * quarter, dcols), BF16),
            pltpu.VMEM((2, slots, quarter, dcols), BF16),
            pltpu.VMEM((2, slots, quarter, dcols), BF16),
            pltpu.VMEM((quarter, width), F32),
            pltpu.VMEM((quarter, width), BF16),
            pltpu.VMEM((quarter, width), BF16),
            dma((2, 3, len(WAYS))), dma((2, 3, len(WAYS))),
            dma((2, 5)), dma((2, 5)),
            dma((2, 7)), dma((2, 7)),
            dma((2, 3, slots)), dma((2, 3, slots)),
            dma((1,)), dma((1,)),
            dma((14,)),
        ],
        compiler_params=pltpu.CompilerParams(
            collective_id=0, has_side_effects=True, vmem_limit_bytes=60 * 1024 * 1024
        ),
    )(
        tokens, mixer_out,
        gate_first, up_first, leftovers(gate_first, up_first), down_first,
        gate_second, up_second, leftovers(gate_second, up_second), down_second,
        vec(gain_first), vec(bias_first), vec(gain_middle), vec(bias_middle), vec(gain_last), vec(bias_last),
    )


def split(hidden):
    main = hidden // 4 // 128 * 128
    return main, hidden // 4 - main


def on_mesh(mesh, rows, width, hidden):
    sizes = dict(mesh.shape)
    if (sizes["rep"], sizes["fs"], sizes["tp"]) != (2, ZS * YS, 2):
        return False
    rows, ks, hidden = rows // (2 * ZS * YS), width // (ZS * YS), hidden // 2
    main, extra = split(hidden)
    return rows % 32 == 0 and ks % 256 == 0 and hidden % 128 == 0 and main > 0 and extra > 0 and extra % 32 == 0


def solution(mesh):
    def run(tokens, mixer_out, gate_first, *rest):
        fits = on_mesh(mesh, tokens.shape[0], tokens.shape[1], gate_first.shape[1])
        return jax.shard_map(
            per_device if fits else per_device_general,
            mesh=mesh,
            in_specs=(
                P(("rep", "fs"), None), P(("rep", "fs"), None),
                P("fs", "tp"), P("fs", "tp"), P("tp", "fs"),
                P("fs", "tp"), P("fs", "tp"), P("tp", "fs"),
                P(), P(), P(), P(), P(), P(),
            ),
            out_specs=P(("rep", "fs"), None),
            check_vma=False,
        )(tokens, mixer_out, gate_first, *rest)

    return run
```

time: 194 us -> 202 us (1.041)
  Pallas kernels: 185 us -> 192 us
    pallas_call x1, Pallas kernels: 185 us -> 192 us  [per_device(): pl.pallas_call(kernel, out_shape=jax.ShapeDtypeStruct((rows, width), BF16...]
    slice x4, local copies, waits for them, and re-layouts: 1.87 us -> 4.44 us  [part(): w[h * (ks // 2):(h + 1) * (ks // 2), 4 * main + q * extra:4 * main + (q +...]
where the time goes in v1:
time: 202 us
  Pallas kernels  192 us (95%)
  local copies, waits for them, and re-layouts  6.96 us (3%)
  other arithmetic  2.28 us (1%)
    pallas_call x1, Pallas kernels, per_device(): pl.pallas_call(kernel, out_shape=jax.ShapeDtypeStruct((rows, width), BF16...  192 us
    slice x4, local copies, waits for them, and re-layouts, part(): w[h * (ks // 2):(h + 1) * (ks // 2), 4 * main + q * extra:4 * main + (q +...  4.44 us

profile of v1, /device:TPU:0, one launch (start us, length us, event | category | flops | bytes accessed | tf_op | source)
XLA Modules:
  0.0 201.5 jit_solution(15157998734678402754)
XLA Ops:
  0.0 1.1 fusion.2
  1.1 1.1 fusion.3
  2.2 0.2 maximum_bitcast_fusion
  2.4 0.2 maximum_bitcast_fusion.2
  2.6 0.8 pad_maximum_fusion.e1_ref
  3.4 1.1 fusion
  4.5 1.1 fusion.1
  5.6 0.2 maximum_bitcast_fusion.4
  5.8 0.2 maximum_bitcast_fusion.6
  5.9 0.8 pad_maximum_fusion.1.e2_ref
  6.8 192.3 %shard_map.136 = bf16[320,2048]{1,0:T(8,128)(2,1)} custom-call(bf16[320,2048]{1,0:T(8,128)(2,1)} %tokens_ref.1, bf16[320,2048]{1,0:T(8,128)(2,1)} %mixer_ref.1, bf16[256,1408]{1,0:T(8,128)(2,1)} %g1_ref.1, bf16[256,1408]{1,0:T(8,128)(2,1)} %u1_ref.1, bf16[4,128,384]{2,1,0:T(8,128)(2,1)} %pad_maximum_fusion.e1_ref, bf16[1408,256]{1,0:T(8,128)(2,1)} %d1_ref.1, ...), custom_call_target="tpu_custom_call" | custom-call | tf_op jit(solution)/shard_map/pallas_call | solution.py:490
  199.0 2.5 %copy.16 = bf16[320,2048]{1,0:T(8,128)(2,1)} copy(bf16[320,2048]{1,0:T(8,128)(2,1)} %shard_map.136) | data formatting | bytes 2621440

commit v2 on v1

--- a/solution.py
+++ b/solution.py
@@ -55,10 +55,10 @@
 
 
 def kernel(
-    tokens_ref, mixer_ref, g1_ref, u1_ref, e1_ref, d1_ref, g2_ref, u2_ref, e2_ref, d2_ref,
+    tokens_ref, mixer_ref, g1_ref, u1_ref, d1_ref, g2_ref, u2_ref, d2_ref,
     gain1_ref, bias1_ref, gain2_ref, bias2_ref, gain3_ref, bias3_ref,
     out_ref,
-    gum, gux, dn, xb, acc, low, high, hid, keep, psend, precv, xsend, xrecv, ysend, yrecv, br, mix, fin,
+    gum, gux, raw, packed, dn, xb, acc, low, high, hid, keep, psend, precv, xsend, xrecv, ysend, yrecv, br, mix, fin,
     zs_send, zs_recv, ys_send, ys_recv, ag_send, ag_recv, rs_send, rs_recv, fin_send, fin_recv, local,
 ):
     rep, fs, core = lax.axis_index("rep"), lax.axis_index("fs"), lax.axis_index("tp")
@@ -82,29 +82,34 @@
         return pl.ds(pl.multiple_of(first, unit), count)
 
     mine, sib = ds(core * quarter, quarter, quarter), ds((1 - core) * quarter, quarter, quarter)
-    weights = ((g1_ref, u1_ref, e1_ref, d1_ref), (g2_ref, u2_ref, e2_ref, d2_ref))
+    weights = ((g1_ref, u1_ref, d1_ref), (g2_ref, u2_ref, d2_ref))
 
     def pieces(f, q):
-        gate, up, ex, down = weights[f]
+        gate, up, down = weights[f]
         rows, mrows, ex_rows = ds(y * ks, ks, ks), ds(q * main, main, main), ds(4 * main + q * extra, extra, 32)
         return (
             (gate.at[:, ds(q * main, main, main)], gum.at[f, 0, rows, pl.ds(0, main)]),
             (up.at[:, ds(q * main, main, main)], gum.at[f, 0, rows, pl.ds(main, main)]),
-            (ex.at[q], gux.at[f, 0, ds(y * fold, fold, fold)]),
+            (packed.at[f], gux.at[f, 0, ds(y * fold, fold, fold)]),
             (down.at[mrows], dn.at[f, y, pl.ds(0, main)]),
             (down.at[ex_rows], dn.at[f, y, pl.ds(main, extra)]),
         )
 
     loads = [
-        [pltpu.make_async_copy(src, dst, local.at[5 * f + i]) for i, (src, dst) in enumerate(pieces(f, own_q))]
+        [
+            pltpu.make_async_copy(src, dst, local.at[6 * f + i])
+            for i, (src, dst) in enumerate([pieces(f, own_q)[i] for i in (0, 1, 3, 4)] + [
+                (w.at[:, pl.ds(4 * main, 4 * extra)], raw.at[f, i]) for i, w in enumerate(weights[f][:2])
+            ])
+        ]
         for f in range(2)
     ]
     token_loads = [
-        pltpu.make_async_copy(tokens_ref.at[mine], xb.at[0, pl.ds(0, quarter)], local.at[10]),
-        pltpu.make_async_copy(tokens_ref.at[sib], xb.at[0, pl.ds(half, quarter)], local.at[11]),
+        pltpu.make_async_copy(tokens_ref.at[mine], xb.at[0, pl.ds(0, quarter)], local.at[12]),
+        pltpu.make_async_copy(tokens_ref.at[sib], xb.at[0, pl.ds(half, quarter)], local.at[13]),
     ]
-    mixer_load = pltpu.make_async_copy(mixer_ref.at[mine], mix, local.at[12])
-    for load in loads[0][:3] + token_loads + loads[0][3:] + loads[1] + [mixer_load]:
+    mixer_load = pltpu.make_async_copy(mixer_ref.at[mine], mix, local.at[14])
+    for load in loads[0][:2] + loads[0][4:] + token_loads + loads[0][2:4] + loads[1] + [mixer_load]:
         load.start()
 
     barrier = pltpu.get_barrier_semaphore()
@@ -196,24 +201,50 @@
     def gets_dn(d):
         return z + d <= ZS - 1
 
-    def own_send(f, which, dy):
+    def own_send(f, which, dy, who=True):
         for way, does in (("up", sends_up), ("dn", sends_dn)):
-            @pl.when(does(1))
+            @pl.when(jnp.logical_and(does(1), who))
             def _():
                 for piece in which:
                     z_copy(f, piece, (way, 1, dy)).start()
 
-    def relay(f, which, d, dys=range(YS)):
+    def own_all(f):
+        for which in (GATE_UP, (DOWN,)):
+            for dy in range(YS):
+                own_send(f, which, dy, jnp.logical_not(inner))
+
+    def forward(f, which, d, dys=range(YS)):
         for dy in dys:
             for way, gets, does in (("up", gets_up, sends_up), ("dn", gets_dn, sends_dn)):
-                @pl.when(gets(d))
+                @pl.when(jnp.logical_and(inner, gets(d)))
                 def _():
                     for piece in which:
                         z_copy(f, piece, (way, d, dy)).wait_recv()
-                        if d < ZS - 1:
-                            @pl.when(does(d + 1))
-                            def _():
-                                z_copy(f, piece, (way, d + 1, dy)).start()
+                        @pl.when(does(d + 1))
+                        def _():
+                            z_copy(f, piece, (way, d + 1, dy)).start()
+
+    def arrive(f, which, d, dys=range(YS)):
+        for way, end in (("up", ZS - 1), ("dn", 0)):
+            @pl.when(z == end)
+            def _():
+                for dy in dys:
+                    for piece in which:
+                        z_copy(f, piece, (way, d, dy)).wait_recv()
+
+    def pack(f):
+        lane = lax.broadcasted_iota(jnp.int32, (fold, 4 * extra), 1)
+
+        def made(q):
+            out = None
+            for p in range(4):
+                part = raw[f, p % 2, (p // 2) * fold:(p // 2 + 1) * fold, :].astype(F32)
+                part = pltpu.roll(part, lax.rem(p - q + 4, 4) * extra, axis=1)
+                out = part if p == 0 else jnp.where(lane < p * extra, out, part)
+            return out.astype(BF16)
+
+        packed[f] = made(pair_q)
+        gux[f, 0, ds(y * fold, fold, fold), :] = made(own_q)
 
     def gather(f, i):
         target = (near, far, far)[i] if i < 3 else other_core
@@ -299,9 +330,9 @@
         shift = 2 * extra - (4 * extra - wide)
         some = -(-extra // 128) * 128
 
-        @pl.loop(0, 8 * quarter // 32)
+        @pl.loop(0, 8)
         def _(i):
-            rows = ds(i * 32, 32, 32)
+            rows = ds(i * quarter, quarter, quarter)
             hid[rows, :main] = gated(acc[rows, :main], acc[rows, main:]).astype(BF16)
             rest = low[rows, :] + pltpu.roll(high[rows, :], wide - shift, axis=1)
             value = pltpu.roll(rest, wide - extra, axis=1)
@@ -346,14 +377,28 @@
         cols = ds(((z + dz) * YS + ya) * dcols, dcols, dcols)
         br[:, cols] = keep[n, :quarter, :] + yrecv[f, n].astype(F32)
 
-    def down(f, d):
-        both(d, lambda dz, ya: down_slot(f, dz, ya))
-        both(d, lambda dz, ya: add_cores(f, dz, ya))
+    groups = [(d, dy) for d in range(ZS) for dy in range(YS)]
+
+    def reduce(f, extra_work):
+        def each(i, act):
+            if 0 <= i < len(groups):
+                d, dy = groups[i]
+                at_distance(d, lambda dz: act(f, dz, lax.rem(y + dy, YS)))
+
+        for i in range(len(groups) + 5):
+            if i < len(groups) and groups[i][0]:
+                arrive(f, (DOWN,), groups[i][0], (groups[i][1],))
+            each(i, down_slot)
+            each(i - 1, add_cores)
+            each(i - 3, add_far)
+            each(i - 5, add_near)
+            if i in extra_work:
+                extra_work[i]()
 
     def first_norms():
-        @pl.loop(0, quarter // 16)
+        @pl.loop(0, quarter // 32)
         def _(i):
-            rows = ds(i * 16, 16, 16)
+            rows = ds(i * 32, 32, 32)
             first = normalize(
                 residual_scale * xb[0, rows, :].astype(F32) + 0.5 * br[rows, :], gain1_ref[...], bias1_ref[...]
             ).astype(BF16)
@@ -362,9 +407,9 @@
             ).astype(BF16)
 
     def last_norm():
-        @pl.loop(0, quarter // 16)
+        @pl.loop(0, quarter // 32)
         def _(i):
-            rows = ds(i * 16, 16, 16)
+            rows = ds(i * 32, 32, 32)
             fin[rows, :] = normalize(
                 residual_scale * xb[1, rows, :].astype(F32) + 0.5 * br[rows, :], gain3_ref[...], bias3_ref[...]
             ).astype(BF16)
@@ -373,75 +418,72 @@
         for i in which:
             loads[f][i].wait()
 
-    pair_start(0, range(3))
-    load_wait(0, range(3))
-    own_send(0, GATE_UP, 0)
+    outer = jnp.logical_not(inner)
+    pair_start(0, (0, 1))
+    load_wait(0, (0, 1))
+    own_send(0, (MAIN,), 0)
+    load_wait(0, (4, 5))
+    pack(0)
+    pair_start(0, (2,))
+    own_send(0, (EXTRA,), 0)
     token_loads[0].wait()
     gather_start(0)
     pair_start(0, (3, 4))
-    load_wait(0, (3, 4))
+    load_wait(0, (2, 3))
     own_send(0, (DOWN,), 0)
+    load_wait(1, range(6))
+    pack(1)
     pair_wait(0, range(3))
     own_send(0, GATE_UP, 1)
-    relay(0, GATE_UP, 1, (0,))
+    forward(0, GATE_UP, 1, (0,))
     gather_near(0)
-    relay(0, GATE_UP, 1, (1,))
+    forward(0, GATE_UP, 1, (1,))
     gather_far(0)
-    pair_start(1, range(3))
+    forward(0, GATE_UP, 2, (0,))
+    pair_start(1, range(5))
+    pair_wait(0, (3, 4))
+    own_send(0, (DOWN,), 1, outer)
     token_loads[1].wait()
     gather_wait(0)
     gate_up(0, 0, first=True)
-    relay(0, GATE_UP, 2, (0,))
+    forward(0, GATE_UP, 2, (1,))
+    arrive(0, GATE_UP, 1)
     at_distance(1, lambda dz: gate_up(0, dz))
-    relay(0, GATE_UP, 2, (1,))
-    pair_wait(0, (3, 4))
-    own_send(0, (DOWN,), 1)
-    relay(0, (DOWN,), 1)
-    pair_start(1, (3, 4))
+    own_send(0, (DOWN,), 1, inner)
+    arrive(0, GATE_UP, 2)
     at_distance(2, lambda dz: gate_up(0, dz))
-    relay(0, GATE_UP, 3)
+    pair_wait(1, range(5))
+    own_all(1)
+    arrive(0, GATE_UP, 3)
     at_distance(3, lambda dz: gate_up(0, dz))
-    relay(0, (DOWN,), 2)
-    load_wait(1, range(5))
-    own_send(1, GATE_UP, 0)
-    pair_wait(1, range(3))
-    own_send(1, GATE_UP, 1)
-    for f in range(2):
-        activate()
-        down(f, 0)
-        down(f, 1)
-        both(0, lambda dz, ya: add_far(f, dz, ya))
-        down(f, 2)
-        both(1, lambda dz, ya: add_far(f, dz, ya))
-        both(0, lambda dz, ya: add_near(f, dz, ya))
-        relay(f, (DOWN,), 3)
-        down(f, 3)
-        both(2, lambda dz, ya: add_far(f, dz, ya))
-        both(1, lambda dz, ya: add_near(f, dz, ya))
-        both(3, lambda dz, ya: add_far(f, dz, ya))
-        both(2, lambda dz, ya: add_near(f, dz, ya))
-        both(3, lambda dz, ya: add_near(f, dz, ya))
-        if f == 0:
-            mixer_load.wait()
-            first_norms()
-            gather_start(1)
-            relay(1, GATE_UP, 1)
-            gather_near(1)
-            relay(1, GATE_UP, 2)
-            own_send(1, (DOWN,), 0)
-            pair_wait(1, (3, 4))
-            own_send(1, (DOWN,), 1)
-            gather_far(1)
-            gather_wait(1)
-            gate_up(1, 0, first=True)
-            at_distance(1, lambda dz: gate_up(1, dz))
-            relay(1, (DOWN,), 1)
-            at_distance(2, lambda dz: gate_up(1, dz))
-            relay(1, (DOWN,), 2)
-            relay(1, GATE_UP, 3)
-            at_distance(3, lambda dz: gate_up(1, dz))
+    activate()
+    forward(0, (DOWN,), 1)
+    forward(0, (DOWN,), 2)
+    own_send(1, GATE_UP, 0, inner)
+    own_send(1, GATE_UP, 1, inner)
+    reduce(0, {6: lambda: forward(1, GATE_UP, 1)})
+    mixer_load.wait()
+    first_norms()
+    gather_start(1)
+    forward(1, GATE_UP, 2)
+    own_send(1, (DOWN,), 0, inner)
+    own_send(1, (DOWN,), 1, inner)
+    gather_near(1)
+    forward(1, (DOWN,), 1)
+    gather_far(1)
+    forward(1, (DOWN,), 2)
+    gather_wait(1)
+    gate_up(1, 0, first=True)
+    arrive(1, GATE_UP, 1)
+    at_distance(1, lambda dz: gate_up(1, dz))
+    arrive(1, GATE_UP, 2)
+    at_distance(2, lambda dz: gate_up(1, dz))
+    arrive(1, GATE_UP, 3)
+    at_distance(3, lambda dz: gate_up(1, dz))
+    activate()
+    reduce(1, {})
     last_norm()
-    put = pltpu.make_async_copy(fin, out_ref.at[mine], local.at[13])
+    put = pltpu.make_async_copy(fin, out_ref.at[mine], local.at[15])
     put.start()
     over = remote(fin, out_ref.at[mine], fin_send.at[0], fin_recv.at[0], other_core)
     over.start()
@@ -476,25 +518,19 @@
     wide = -(-2 * extra // 128) * 128
     slots = ZS * YS
 
-    def leftovers(gate, up):
-        def part(w, h, q):
-            return w[h * (ks // 2):(h + 1) * (ks // 2), 4 * main + q * extra:4 * main + (q + 1) * extra]
-
-        return jnp.stack([
-            jnp.concatenate([part(w, h, q) for h in range(2) for w in (gate, up)], axis=1) for q in range(4)
-        ])
-
     any_spec, vmem = pl.BlockSpec(memory_space=pl.ANY), pl.BlockSpec(memory_space=pltpu.VMEM)
     vec = lambda v: v.reshape(1, width)
     dma = pltpu.SemaphoreType.DMA
     return pl.pallas_call(
         kernel,
         out_shape=jax.ShapeDtypeStruct((rows, width), BF16),
-        in_specs=[any_spec] * 10 + [vmem] * 6,
+        in_specs=[any_spec] * 8 + [vmem] * 6,
         out_specs=any_spec,
         scratch_shapes=[
             pltpu.VMEM((2, ZS, YS * ks, 2 * main), BF16),
             pltpu.VMEM((2, ZS, YS * ks // 2, 4 * extra), BF16),
+            pltpu.VMEM((2, 2, ks, 4 * extra), BF16),
+            pltpu.VMEM((2, ks // 2, 4 * extra), BF16),
             pltpu.VMEM((2, slots, main + extra, dcols), BF16),
             pltpu.VMEM((2, 8 * quarter, width), BF16),
             pltpu.VMEM((8 * quarter, 2 * main), F32),
@@ -516,15 +552,14 @@
             dma((2, 7)), dma((2, 7)),
             dma((2, 3, slots)), dma((2, 3, slots)),
             dma((1,)), dma((1,)),
-            dma((14,)),
+            dma((16,)),
         ],
         compiler_params=pltpu.CompilerParams(
             collective_id=0, has_side_effects=True, vmem_limit_bytes=60 * 1024 * 1024
         ),
     )(
         tokens, mixer_out,
-        gate_first, up_first, leftovers(gate_first, up_first), down_first,
-        gate_second, up_second, leftovers(gate_second, up_second), down_second,
+        gate_first, up_first, down_first, gate_second, up_second, down_second,
         vec(gain_first), vec(bias_first), vec(gain_middle), vec(bias_middle), vec(gain_last), vec(bias_last),
     )
 

time: 202 us -> 167 us (0.83)
  Pallas kernels: 192 us -> 164 us
  local copies, waits for them, and re-layouts: 6.96 us -> 2.52 us
  other arithmetic: 2.28 us -> 0 us
    pallas_call x1, Pallas kernels: 192 us -> 164 us  [per_device(): pl.pallas_call(kernel, out_shape=jax.ShapeDtypeStruct((rows, width), BF16...]
    slice x4 -> x0, local copies, waits for them, and re-layouts: 4.44 us -> none  [part(): w[h * (ks // 2):(h + 1) * (ks // 2), 4 * main + q * extra:4 * main + (q +...]
    another operation x6 -> x0, other arithmetic: 2.28 us -> none  [leftovers(): jnp.stack([jnp.concatenate([part(w, h, q) for h in range(2) for w in (gat...]
where the time goes in v2:
time: 167 us
  Pallas kernels  164 us (98%)
  local copies, waits for them, and re-layouts  2.52 us (2%)
    pallas_call x1, Pallas kernels, per_device(): pl.pallas_call(kernel, out_shape=jax.ShapeDtypeStruct((rows, width), BF16...  164 us

profile of v2, /device:TPU:0, one launch (start us, length us, event | category | flops | bytes accessed | tf_op | source)
XLA Modules:
  0.0 166.9 jit_solution(10810631093103256862)
XLA Ops:
  0.0 164.3 %shard_map.136 = bf16[320,2048]{1,0:T(8,128)(2,1)} custom-call(bf16[320,2048]{1,0:T(8,128)(2,1)} %tokens_ref.1, bf16[320,2048]{1,0:T(8,128)(2,1)} %mixer_ref.1, bf16[256,1408]{1,0:T(8,128)(2,1)} %g1_ref.1, bf16[256,1408]{1,0:T(8,128)(2,1)} %u1_ref.1, bf16[1408,256]{1,0:T(8,128)(2,1)} %d1_ref.1, bf16[256,1408]{1,0:T(8,128)(2,1)} %g2_ref.1, ...), custom_call_target="tpu_custom_call" | custom-call | tf_op jit(solution)/shard_map/pallas_call | solution.py:524
  164.3 2.5 %copy.16 = bf16[320,2048]{1,0:T(8,128)(2,1)} copy(bf16[320,2048]{1,0:T(8,128)(2,1)} %shard_map.136) | data formatting | bytes 2621440

commit v3 on v2

--- a/solution.py
+++ b/solution.py
@@ -54,16 +54,20 @@
 GATE_UP = (MAIN, EXTRA)
 
 
+FIRST_ORDER = "D0 D1 C0 D2 C1 D3 C2 F0 D4 C3 F1 D5 C4 F2 N0 D6 C5 F3 N1 D7 C6 F4 N2 C7 F5 N3 F6 N4 F7 N5 N6 N7"
+LAST_ORDER = "D0 D1 C0 D2 C1 D3 C2 F0 C3 F1 D4 C4 F2 D5 C5 F3 D6 C6 F4 D7 C7 F5 N0 N1 N2 F6 N3 N4 F7 N5 N6 N7"
+
+
 def kernel(
     tokens_ref, mixer_ref, g1_ref, u1_ref, d1_ref, g2_ref, u2_ref, d2_ref,
-    gain1_ref, bias1_ref, gain2_ref, bias2_ref, gain3_ref, bias3_ref,
+    gain1_hbm, bias1_hbm, gain2_hbm, bias2_hbm, gain3_hbm, bias3_hbm,
     out_ref,
-    gum, gux, raw, packed, dn, xb, acc, low, high, hid, keep, psend, precv, xsend, xrecv, ysend, yrecv, br, mix, fin,
+    vecs, gum, gux, raw, packed, dn, xb, acc, low, high, hid, keep, psend, precv, xsend, xrecv, ysend, yrecv, br, mix,
     zs_send, zs_recv, ys_send, ys_recv, ag_send, ag_recv, rs_send, rs_recv, fin_send, fin_recv, local,
 ):
     rep, fs, core = lax.axis_index("rep"), lax.axis_index("fs"), lax.axis_index("tp")
     z, y = fs // YS, fs % YS
-    quarter = fin.shape[0]
+    quarter = br.shape[0]
     half = 4 * quarter
     ks = gum.shape[2] // YS
     main = gum.shape[3] // 2
@@ -108,8 +112,12 @@
         pltpu.make_async_copy(tokens_ref.at[mine], xb.at[0, pl.ds(0, quarter)], local.at[12]),
         pltpu.make_async_copy(tokens_ref.at[sib], xb.at[0, pl.ds(half, quarter)], local.at[13]),
     ]
+    vec_loads = [
+        pltpu.make_async_copy(src, vecs.at[i], local.at[15 + i])
+        for i, src in enumerate((gain1_hbm, bias1_hbm, gain2_hbm, bias2_hbm, gain3_hbm, bias3_hbm))
+    ]
     mixer_load = pltpu.make_async_copy(mixer_ref.at[mine], mix, local.at[14])
-    for load in loads[0][:2] + loads[0][4:] + token_loads + loads[0][2:4] + loads[1] + [mixer_load]:
+    for load in loads[0][:2] + loads[0][4:] + token_loads + loads[0][2:4] + loads[1] + [mixer_load] + vec_loads:
         load.start()
 
     barrier = pltpu.get_barrier_semaphore()
@@ -379,46 +387,85 @@
 
     groups = [(d, dy) for d in range(ZS) for dy in range(YS)]
 
-    def reduce(f, extra_work):
-        def each(i, act):
-            if 0 <= i < len(groups):
-                d, dy = groups[i]
-                at_distance(d, lambda dz: act(f, dz, lax.rem(y + dy, YS)))
-
-        for i in range(len(groups) + 5):
-            if i < len(groups) and groups[i][0]:
-                arrive(f, (DOWN,), groups[i][0], (groups[i][1],))
-            each(i, down_slot)
-            each(i - 1, add_cores)
-            each(i - 3, add_far)
-            each(i - 5, add_near)
-            if i in extra_work:
-                extra_work[i]()
+    stages = {"C": add_cores, "F": add_far, "N": add_near}
+
+    def reduce(f, order, extra_work):
+        for i, name in enumerate(order.split()):
+            d, dy = groups[int(name[1])]
+            act = stages.get(name[0], down_slot)
+            if act is down_slot and d:
+                arrive(f, (DOWN,), d, (dy,))
+            at_distance(d, lambda dz: act(f, dz, lax.rem(y + dy, YS)))
+            if name in extra_work:
+                extra_work[name]()
 
     def first_norms():
         @pl.loop(0, quarter // 32)
         def _(i):
             rows = ds(i * 32, 32, 32)
             first = normalize(
-                residual_scale * xb[0, rows, :].astype(F32) + 0.5 * br[rows, :], gain1_ref[...], bias1_ref[...]
+                residual_scale * xb[0, rows, :].astype(F32) + 0.5 * br[rows, :], vecs[0], vecs[1]
             ).astype(BF16)
             xb[1, rows, :] = normalize(
-                residual_scale * first.astype(F32) + mix[rows, :].astype(F32), gain2_ref[...], bias2_ref[...]
+                residual_scale * first.astype(F32) + mix[rows, :].astype(F32), vecs[2], vecs[3]
             ).astype(BF16)
+
+    def out_copy(i):
+        rows = ds(core * quarter + i * 32, 32, 32)
+        return remote(out_ref.at[rows], out_ref.at[rows], fin_send.at[i], fin_recv.at[i], other_core)
 
     def last_norm():
         @pl.loop(0, quarter // 32)
         def _(i):
             rows = ds(i * 32, 32, 32)
-            fin[rows, :] = normalize(
-                residual_scale * xb[1, rows, :].astype(F32) + 0.5 * br[rows, :], gain3_ref[...], bias3_ref[...]
+            out_ref[ds(core * quarter + i * 32, 32, 32), :] = normalize(
+                residual_scale * xb[1, rows, :].astype(F32) + 0.5 * br[rows, :], vecs[4], vecs[5]
             ).astype(BF16)
+            out_copy(i).start()
+
+    def sent_wait():
+        for copy in sent:
+            copy.wait_send()
+        sent.clear()
+
+    def z_sent_wait(f):
+        for d in STEPS:
+            for way, does in (("up", sends_up), ("dn", sends_dn)):
+                @pl.when(does(d))
+                def _():
+                    for piece in range(3):
+                        for dy in range(YS):
+                            z_copy(f, piece, (way, d, dy)).wait_send()
+
+    def reduce_sent_wait(f):
+        @pl.loop(0, ZS * YS)
+        def _(n):
+            for copy in (to_sibling(f, n), to_far(f, n), to_near(f, n)):
+                copy.wait_send()
 
     def load_wait(f, which):
         for i in which:
             loads[f][i].wait()
 
     outer = jnp.logical_not(inner)
+
+    def outer_middle():
+        @pl.when(outer)
+        def _():
+            pair_wait(1, range(5))
+
+        own_all(1)
+
+    def inner_middle():
+        forward(0, (DOWN,), 2)
+
+        @pl.when(inner)
+        def _():
+            pair_wait(1, range(5))
+
+        own_send(1, GATE_UP, 0, inner)
+        own_send(1, GATE_UP, 1, inner)
+
     pair_start(0, (0, 1))
     load_wait(0, (0, 1))
     own_send(0, (MAIN,), 0)
@@ -452,58 +499,41 @@
     own_send(0, (DOWN,), 1, inner)
     arrive(0, GATE_UP, 2)
     at_distance(2, lambda dz: gate_up(0, dz))
-    pair_wait(1, range(5))
-    own_all(1)
+    outer_middle()
     arrive(0, GATE_UP, 3)
     at_distance(3, lambda dz: gate_up(0, dz))
     activate()
     forward(0, (DOWN,), 1)
-    forward(0, (DOWN,), 2)
-    own_send(1, GATE_UP, 0, inner)
-    own_send(1, GATE_UP, 1, inner)
-    reduce(0, {6: lambda: forward(1, GATE_UP, 1)})
-    mixer_load.wait()
+    reduce(0, FIRST_ORDER, {"D3": inner_middle, "F3": lambda: forward(1, GATE_UP, 1)})
+    for load in [mixer_load] + vec_loads:
+        load.wait()
     first_norms()
     gather_start(1)
+    gather_near(1)
     forward(1, GATE_UP, 2)
     own_send(1, (DOWN,), 0, inner)
     own_send(1, (DOWN,), 1, inner)
-    gather_near(1)
-    forward(1, (DOWN,), 1)
     gather_far(1)
-    forward(1, (DOWN,), 2)
     gather_wait(1)
     gate_up(1, 0, first=True)
+    forward(1, (DOWN,), 1)
     arrive(1, GATE_UP, 1)
     at_distance(1, lambda dz: gate_up(1, dz))
+    forward(1, (DOWN,), 2)
     arrive(1, GATE_UP, 2)
     at_distance(2, lambda dz: gate_up(1, dz))
+    sent_wait()
+    z_sent_wait(0)
+    reduce_sent_wait(0)
     arrive(1, GATE_UP, 3)
     at_distance(3, lambda dz: gate_up(1, dz))
     activate()
-    reduce(1, {})
+    reduce(1, LAST_ORDER, {"F7": lambda: z_sent_wait(1)})
+    reduce_sent_wait(1)
     last_norm()
-    put = pltpu.make_async_copy(fin, out_ref.at[mine], local.at[15])
-    put.start()
-    over = remote(fin, out_ref.at[mine], fin_send.at[0], fin_recv.at[0], other_core)
-    over.start()
-    over.wait()
-    put.wait()
-    for copy in sent:
-        copy.wait_send()
-    for f in range(2):
-        @pl.loop(0, ZS * YS)
-        def _(n):
-            for copy in (to_sibling(f, n), to_far(f, n), to_near(f, n)):
-                copy.wait_send()
-
-        for d in STEPS:
-            for way, does in (("up", sends_up), ("dn", sends_dn)):
-                @pl.when(does(d))
-                def _():
-                    for piece in range(3):
-                        for dy in range(YS):
-                            z_copy(f, piece, (way, d, dy)).wait_send()
+    @pl.loop(0, quarter // 32)
+    def _(i):
+        out_copy(i).wait()
 
 
 def per_device(
@@ -523,10 +553,11 @@
     dma = pltpu.SemaphoreType.DMA
     return pl.pallas_call(
         kernel,
-        out_shape=jax.ShapeDtypeStruct((rows, width), BF16),
-        in_specs=[any_spec] * 8 + [vmem] * 6,
-        out_specs=any_spec,
+        out_shape=pltpu.VMEM((rows, width), BF16),
+        in_specs=[any_spec] * 14,
+        out_specs=pl.BlockSpec(memory_space=pltpu.VMEM),
         scratch_shapes=[
+            pltpu.VMEM((6, 1, width), F32),
             pltpu.VMEM((2, ZS, YS * ks, 2 * main), BF16),
             pltpu.VMEM((2, ZS, YS * ks // 2, 4 * extra), BF16),
             pltpu.VMEM((2, 2, ks, 4 * extra), BF16),
@@ -546,13 +577,12 @@
             pltpu.VMEM((2, slots, quarter, dcols), BF16),
             pltpu.VMEM((quarter, width), F32),
             pltpu.VMEM((quarter, width), BF16),
-            pltpu.VMEM((quarter, width), BF16),
             dma((2, 3, len(WAYS))), dma((2, 3, len(WAYS))),
             dma((2, 5)), dma((2, 5)),
             dma((2, 7)), dma((2, 7)),
             dma((2, 3, slots)), dma((2, 3, slots)),
-            dma((1,)), dma((1,)),
-            dma((16,)),
+            dma((quarter // 32,)), dma((quarter // 32,)),
+            dma((21,)),
         ],
         compiler_params=pltpu.CompilerParams(
             collective_id=0, has_side_effects=True, vmem_limit_bytes=60 * 1024 * 1024

time: 167 us -> 162 us (0.970)
  Pallas kernels: 164 us -> 161 us
    pallas_call x1, Pallas kernels: 164 us -> 161 us  [per_device(): pl.pallas_call(kernel, out_shape=pltpu.VMEM((rows, width), BF16), in_spec...]
where the time goes in v3:
time: 162 us
  Pallas kernels  161 us (99%)
    pallas_call x1, Pallas kernels, per_device(): pl.pallas_call(kernel, out_shape=pltpu.VMEM((rows, width), BF16), in_spec...  161 us

profile of v3, /device:TPU:0, one launch (start us, length us, event | category | flops | bytes accessed | tf_op | source)
XLA Modules:
  0.0 162.2 jit_solution(13841701546599542526)
XLA Ops:
  0.0 161.1 %shard_map.136 = bf16[320,2048]{1,0:T(8,128)(2,1)S(1)} custom-call(bf16[320,2048]{1,0:T(8,128)(2,1)} %tokens_ref.1, bf16[320,2048]{1,0:T(8,128)(2,1)} %mixer_ref.1, bf16[256,1408]{1,0:T(8,128)(2,1)} %g1_ref.1, bf16[256,1408]{1,0:T(8,128)(2,1)} %u1_ref.1, bf16[1408,256]{1,0:T(8,128)(2,1)} %d1_ref.1, bf16[256,1408]{1,0:T(8,128)(2,1)} %g2_ref.1, ...), custom_call_target="tpu_custom_call" | custom-call | tf_op jit(solution)/shard_map/pallas_call | solution.py:554
  161.1 1.1 copy.16

commit v4 on v3

--- a/solution.py
+++ b/solution.py
@@ -49,7 +49,6 @@
 
 
 STEPS = range(1, ZS)
-WAYS = [(way, d, dy) for way in ("up", "dn") for d in STEPS for dy in range(YS)]
 MAIN, EXTRA, DOWN = range(3)
 GATE_UP = (MAIN, EXTRA)
 
@@ -63,7 +62,7 @@
     gain1_hbm, bias1_hbm, gain2_hbm, bias2_hbm, gain3_hbm, bias3_hbm,
     out_ref,
     vecs, gum, gux, raw, packed, dn, xb, acc, low, high, hid, keep, psend, precv, xsend, xrecv, ysend, yrecv, br, mix,
-    zs_send, zs_recv, ys_send, ys_recv, ag_send, ag_recv, rs_send, rs_recv, fin_send, fin_recv, local,
+    zs_send, zs_recv, ys_send, ys_recv, ag_send, ag_recv, rs_send, rs_recv, fin_sem, local,
 ):
     rep, fs, core = lax.axis_index("rep"), lax.axis_index("fs"), lax.axis_index("tp")
     z, y = fs // YS, fs % YS
@@ -101,7 +100,7 @@
 
     loads = [
         [
-            pltpu.make_async_copy(src, dst, local.at[6 * f + i])
+            pltpu.make_async_copy(src, dst, local.at[3 * f + i // 2])
             for i, (src, dst) in enumerate([pieces(f, own_q)[i] for i in (0, 1, 3, 4)] + [
                 (w.at[:, pl.ds(4 * main, 4 * extra)], raw.at[f, i]) for i, w in enumerate(weights[f][:2])
             ])
@@ -109,14 +108,14 @@
         for f in range(2)
     ]
     token_loads = [
-        pltpu.make_async_copy(tokens_ref.at[mine], xb.at[0, pl.ds(0, quarter)], local.at[12]),
-        pltpu.make_async_copy(tokens_ref.at[sib], xb.at[0, pl.ds(half, quarter)], local.at[13]),
+        pltpu.make_async_copy(tokens_ref.at[mine], xb.at[0, pl.ds(0, quarter)], local.at[6]),
+        pltpu.make_async_copy(tokens_ref.at[sib], xb.at[0, pl.ds(half, quarter)], local.at[7]),
     ]
     vec_loads = [
-        pltpu.make_async_copy(src, vecs.at[i], local.at[15 + i])
+        pltpu.make_async_copy(src, vecs.at[i], local.at[9 + i])
         for i, src in enumerate((gain1_hbm, bias1_hbm, gain2_hbm, bias2_hbm, gain3_hbm, bias3_hbm))
     ]
-    mixer_load = pltpu.make_async_copy(mixer_ref.at[mine], mix, local.at[14])
+    mixer_load = pltpu.make_async_copy(mixer_ref.at[mine], mix, local.at[8])
     for load in loads[0][:2] + loads[0][4:] + token_loads + loads[0][2:4] + loads[1] + [mixer_load] + vec_loads:
         load.start()
 
@@ -148,8 +147,6 @@
     @pl.when(jnp.logical_not(inner))
     def _():
         pl.semaphore_wait(barrier, 4)
-
-    sent = []
 
     def remote(src, dst, send_sem, recv_sem, target):
         return pltpu.make_async_remote_copy(
@@ -157,26 +154,20 @@
             device_id=target, device_id_type=pl.DeviceIdType.MESH,
         )
 
-    def send(copy):
-        copy.start()
-        sent.append(copy)
-
     def pair_copy(f, i):
         src, dst = pieces(f, pair_q)[i]
-        return remote(src, dst, ys_send.at[f, i], ys_recv.at[f, i], pair)
+        n = (0, 0, 1, 2, 2)[i]
+        return remote(src, dst, ys_send.at[f, n], ys_recv.at[f, n], pair)
 
     def pair_landing(f, i):
-        gate_rows = ds((1 - y) * ks, ks, ks)
         dst = (
-            gum.at[f, 0, gate_rows, pl.ds(0, main)], gum.at[f, 0, gate_rows, pl.ds(main, main)],
-            gux.at[f, 0, ds((1 - y) * fold, fold, fold)],
-            dn.at[f, 1 - y, pl.ds(0, main)], dn.at[f, 1 - y, pl.ds(main, extra)],
+            gum.at[f, 0, ds((1 - y) * ks, ks, ks)], gux.at[f, 0, ds((1 - y) * fold, fold, fold)], dn.at[f, 1 - y],
         )[i]
         return remote(dst, dst, ys_send.at[f, i], ys_recv.at[f, i], pair)
 
     def pair_start(f, which):
         for i in which:
-            send(pair_copy(f, i))
+            pair_copy(f, i).start()
 
     def pair_wait(f, which):
         for i in which:
@@ -194,8 +185,17 @@
                 return gux.at[f, n, ds(ya * fold, fold, fold)]
             return dn.at[f, n * YS + ya]
 
-        sems = zs_send.at[f, piece, WAYS.index(name)], zs_recv.at[f, piece, WAYS.index(name)]
-        return remote(at(slot_of(sign * (d - 1))), at(slot_of(sign * d)), *sems, plane(-sign))
+        there = slot_of(sign * d)
+        sems = zs_send.at[f, piece, int(way == "up")], zs_recv.at[f, int(piece == DOWN), there - 1, dy]
+        return remote(at(slot_of(sign * (d - 1))), at(there), *sems, plane(-sign))
+
+    def z_wait(f, which, name):
+        way, d, dy = name
+        n = slot_of(-d if way == "up" else d)
+        span = (ks * 2 * main + fold * 4 * extra) // xb.shape[2]
+        landed = dn.at[f, n * YS] if which == (DOWN,) else xb.at[f, pl.ds(0, span)]
+        sem = zs_recv.at[f, int(which == (DOWN,)), n - 1, dy]
+        remote(landed, landed, sem, sem, other_core).wait_recv()
 
     def sends_up(d):
         return jnp.logical_and(z >= d - 1, z < ZS - 1)
@@ -226,10 +226,11 @@
             for way, gets, does in (("up", gets_up, sends_up), ("dn", gets_dn, sends_dn)):
                 @pl.when(jnp.logical_and(inner, gets(d)))
                 def _():
-                    for piece in which:
-                        z_copy(f, piece, (way, d, dy)).wait_recv()
-                        @pl.when(does(d + 1))
-                        def _():
+                    z_wait(f, which, (way, d, dy))
+
+                    @pl.when(does(d + 1))
+                    def _():
+                        for piece in which:
                             z_copy(f, piece, (way, d + 1, dy)).start()
 
     def arrive(f, which, d, dys=range(YS)):
@@ -237,8 +238,7 @@
             @pl.when(z == end)
             def _():
                 for dy in dys:
-                    for piece in which:
-                        z_copy(f, piece, (way, d, dy)).wait_recv()
+                    z_wait(f, which, (way, d, dy))
 
     def pack(f):
         lane = lax.broadcasted_iota(jnp.int32, (fold, 4 * extra), 1)
@@ -260,25 +260,32 @@
         dst = i + 1 if i < 3 else i + 1
         return remote(
             xb.at[f, pl.ds(src * quarter, quarter)], xb.at[f, pl.ds(dst * quarter, quarter)],
-            ag_send.at[f, i], ag_recv.at[f, i], target,
+            ag_send.at[0], ag_recv.at[i], target,
         )
 
+    def gather_send(f, i):
+        gather(f, i).start()
+
+    def gather_sent_wait(f):
+        gone = xb.at[f, pl.ds(0, (6 + f) * quarter)]
+        remote(gone, gone, ag_send.at[0], ag_recv.at[0], other_core).wait_send()
+
     def gather_start(f):
-        send(gather(f, 0))
-        send(gather(f, 1))
+        gather_send(f, 0)
+        gather_send(f, 1)
         if f:
-            send(gather(f, 3))
+            gather_send(f, 3)
 
     def gather_near(f):
         gather(f, 0).wait_recv()
-        send(gather(f, 2))
-        send(gather(f, 4))
+        gather_send(f, 2)
+        gather_send(f, 4)
 
     def gather_far(f):
         gather(f, 1).wait_recv()
-        send(gather(f, 5))
+        gather_send(f, 5)
         gather(f, 2).wait_recv()
-        send(gather(f, 6))
+        gather_send(f, 6)
 
     def gather_wait(f):
         for i in range(3 if f else 4, 7):
@@ -351,13 +358,13 @@
         return lax.rem(dz + ZS, ZS) * YS + ya
 
     def to_sibling(f, n):
-        return remote(psend.at[f, n], precv.at[f, n], rs_send.at[f, 0, n], rs_recv.at[f, 0, n], other_core)
+        return remote(psend.at[f, n], precv.at[f, n], rs_send.at[0], rs_recv.at[0, n], other_core)
 
     def to_far(f, n):
-        return remote(xsend.at[f, n], xrecv.at[f, n], rs_send.at[f, 1, n], rs_recv.at[f, 1, n], far)
+        return remote(xsend.at[f, n], xrecv.at[f, n], rs_send.at[1], rs_recv.at[1, n], far)
 
     def to_near(f, n):
-        return remote(ysend.at[f, n], yrecv.at[f, n], rs_send.at[f, 2, n], rs_recv.at[f, 2, n], near)
+        return remote(ysend.at[f, n], yrecv.at[f, n], rs_send.at[2], rs_recv.at[2, n], near)
 
     def down_slot(f, dz, ya):
         n = index(dz, ya)
@@ -412,7 +419,7 @@
 
     def out_copy(i):
         rows = ds(core * quarter + i * 32, 32, 32)
-        return remote(out_ref.at[rows], out_ref.at[rows], fin_send.at[i], fin_recv.at[i], other_core)
+        return remote(out_ref.at[rows], out_ref.at[rows], fin_sem.at[0], fin_sem.at[1], other_core)
 
     def last_norm():
         @pl.loop(0, quarter // 32)
@@ -423,36 +430,34 @@
             ).astype(BF16)
             out_copy(i).start()
 
-    def sent_wait():
-        for copy in sent:
-            copy.wait_send()
-        sent.clear()
+    def pair_sent_wait(f):
+        for i in range(3):
+            pair_landing(f, i).wait_send()
 
     def z_sent_wait(f):
-        for d in STEPS:
-            for way, does in (("up", sends_up), ("dn", sends_dn)):
-                @pl.when(does(d))
+        for way, sign in (("up", -1), ("dn", 1)):
+            for planes in STEPS:
+                @pl.when(z == (planes - 1 if sign < 0 else ZS - planes))
                 def _():
                     for piece in range(3):
-                        for dy in range(YS):
-                            z_copy(f, piece, (way, d, dy)).wait_send()
+                        gone = (gum, gux, dn)[piece].at[f, pl.ds(0, planes * (YS if piece == DOWN else 1))]
+                        sem = zs_send.at[f, piece, int(way == "up")]
+                        remote(gone, gone, sem, sem, other_core).wait_send()
 
     def reduce_sent_wait(f):
-        @pl.loop(0, ZS * YS)
-        def _(n):
-            for copy in (to_sibling(f, n), to_far(f, n), to_near(f, n)):
-                copy.wait_send()
-
-    def load_wait(f, which):
-        for i in which:
-            loads[f][i].wait()
+        for i, gone in enumerate((psend.at[f], xsend.at[f], ysend.at[f])):
+            remote(gone, gone, rs_send.at[i], rs_send.at[i], other_core).wait_send()
+
+    def load_wait(f, i):
+        landed = (gum.at[f, 0, ds(y * ks, ks, ks)], dn.at[f, y], raw.at[f])[i]
+        pltpu.make_async_copy(landed, landed, local.at[3 * f + i]).wait()
 
     outer = jnp.logical_not(inner)
 
     def outer_middle():
         @pl.when(outer)
         def _():
-            pair_wait(1, range(5))
+            pair_wait(1, range(3))
 
         own_all(1)
 
@@ -461,26 +466,28 @@
 
         @pl.when(inner)
         def _():
-            pair_wait(1, range(5))
+            pair_wait(1, range(3))
 
         own_send(1, GATE_UP, 0, inner)
         own_send(1, GATE_UP, 1, inner)
 
     pair_start(0, (0, 1))
-    load_wait(0, (0, 1))
+    load_wait(0, 0)
     own_send(0, (MAIN,), 0)
-    load_wait(0, (4, 5))
+    load_wait(0, 2)
     pack(0)
     pair_start(0, (2,))
     own_send(0, (EXTRA,), 0)
     token_loads[0].wait()
     gather_start(0)
     pair_start(0, (3, 4))
-    load_wait(0, (2, 3))
+    load_wait(0, 1)
     own_send(0, (DOWN,), 0)
-    load_wait(1, range(6))
+    load_wait(1, 0)
+    load_wait(1, 1)
+    load_wait(1, 2)
     pack(1)
-    pair_wait(0, range(3))
+    pair_wait(0, (0, 1))
     own_send(0, GATE_UP, 1)
     forward(0, GATE_UP, 1, (0,))
     gather_near(0)
@@ -488,7 +495,7 @@
     gather_far(0)
     forward(0, GATE_UP, 2, (0,))
     pair_start(1, range(5))
-    pair_wait(0, (3, 4))
+    pair_wait(0, (2,))
     own_send(0, (DOWN,), 1, outer)
     token_loads[1].wait()
     gather_wait(0)
@@ -508,6 +515,8 @@
     for load in [mixer_load] + vec_loads:
         load.wait()
     first_norms()
+    gather_sent_wait(0)
+    reduce_sent_wait(0)
     gather_start(1)
     gather_near(1)
     forward(1, GATE_UP, 2)
@@ -522,18 +531,18 @@
     forward(1, (DOWN,), 2)
     arrive(1, GATE_UP, 2)
     at_distance(2, lambda dz: gate_up(1, dz))
-    sent_wait()
+    pair_sent_wait(0)
+    pair_sent_wait(1)
     z_sent_wait(0)
-    reduce_sent_wait(0)
     arrive(1, GATE_UP, 3)
     at_distance(3, lambda dz: gate_up(1, dz))
     activate()
     reduce(1, LAST_ORDER, {"F7": lambda: z_sent_wait(1)})
+    gather_sent_wait(1)
     reduce_sent_wait(1)
     last_norm()
-    @pl.loop(0, quarter // 32)
-    def _(i):
-        out_copy(i).wait()
+    gone, landed = out_ref.at[mine], out_ref.at[sib]
+    remote(gone, landed, fin_sem.at[0], fin_sem.at[1], other_core).wait()
 
 
 def per_device(
@@ -577,12 +586,12 @@
             pltpu.VMEM((2, slots, quarter, dcols), BF16),
             pltpu.VMEM((quarter, width), F32),
             pltpu.VMEM((quarter, width), BF16),
-            dma((2, 3, len(WAYS))), dma((2, 3, len(WAYS))),
-            dma((2, 5)), dma((2, 5)),
-            dma((2, 7)), dma((2, 7)),
-            dma((2, 3, slots)), dma((2, 3, slots)),
-            dma((quarter // 32,)), dma((quarter // 32,)),
-            dma((21,)),
+            dma((2, 3, 2)), dma((2, 2, ZS - 1, YS)),
+            dma((2, 3)), dma((2, 3)),
+            dma((1,)), dma((7,)),
+            dma((3,)), dma((3, slots)),
+            dma((2,)),
+            dma((15,)),
         ],
         compiler_params=pltpu.CompilerParams(
             collective_id=0, has_side_effects=True, vmem_limit_bytes=60 * 1024 * 1024
@@ -605,7 +614,9 @@
         return False
     rows, ks, hidden = rows // (2 * ZS * YS), width // (ZS * YS), hidden // 2
     main, extra = split(hidden)
-    return rows % 32 == 0 and ks % 256 == 0 and hidden % 128 == 0 and main > 0 and extra > 0 and extra % 32 == 0
+    span = ks * 2 * (main + extra)
+    fits = rows % 32 == 0 and ks % 256 == 0 and hidden % 128 == 0 and span % (8 * width) == 0
+    return fits and main > 0 and extra > 0 and extra % 32 == 0
 
 
 def solution(mesh):

time: 162 us -> 160 us (0.988)
  Pallas kernels: 161 us -> 159 us
    pallas_call x1, Pallas kernels: 161 us -> 159 us  [per_device(): pl.pallas_call(kernel, out_shape=pltpu.VMEM((rows, width), BF16), in_spec...]
where the time goes in v4:
time: 160 us
  Pallas kernels  159 us (99%)
    pallas_call x1, Pallas kernels, per_device(): pl.pallas_call(kernel, out_shape=pltpu.VMEM((rows, width), BF16), in_spec...  159 us

profile of v4, /device:TPU:0, one launch (start us, length us, event | category | flops | bytes accessed | tf_op | source)
XLA Modules:
  0.0 160.1 jit_solution(2191891800356525978)
XLA Ops:
  0.0 159.1 %shard_map.136 = bf16[320,2048]{1,0:T(8,128)(2,1)S(1)} custom-call(bf16[320,2048]{1,0:T(8,128)(2,1)} %tokens_ref.1, bf16[320,2048]{1,0:T(8,128)(2,1)} %mixer_ref.1, bf16[256,1408]{1,0:T(8,128)(2,1)} %g1_ref.1, bf16[256,1408]{1,0:T(8,128)(2,1)} %u1_ref.1, bf16[1408,256]{1,0:T(8,128)(2,1)} %d1_ref.1, bf16[256,1408]{1,0:T(8,128)(2,1)} %g2_ref.1, ...), custom_call_target="tpu_custom_call" | custom-call | tf_op jit(solution)/shard_map/pallas_call | solution.py:563
  159.1 1.1 copy.16
